TPU v7x, 32 devices: a whole 2x2x4 slice. The times are simulated.
32 devices in a mesh: sp: 8 (over z, y), tp: 4 (over x, core).
Axes of the slice: x: 2, y: 2, z: 4, core: 2. Of those that a mesh axis runs over, the one named last changes fastest.
Arguments:
- latent: bfloat16 [4096, 4096], P(('sp', 'tp')), may hold values from -3 to 3
- context: bfloat16 [1024, 4096], P('sp'), may hold values from -6 to 6
- cond: float32 [4096], replicated, may hold values from -6 to 6
- ctx_cond: float32 [4096], replicated, may hold values from -6 to 6
- w_shift: bfloat16 [4096, 4096], P('sp', 'tp'), may hold values from -0.1875 to 0.1875
- w_scale: bfloat16 [4096, 4096], P('sp', 'tp'), may hold values from -0.09375 to 0.15478516
- w_gate: bfloat16 [4096, 4096], P('sp', 'tp'), may hold values from -0.1875 to 0.1875
- w_query: bfloat16 [4096, 2048], P(None, 'tp'), may hold values from -0.09375 to 0.09375
- key_weight: bfloat16 [4096, 1024], P(None, 'tp'), may hold values from -0.09375 to 0.09375
- value_weight: bfloat16 [4096, 1024], P(None, 'tp'), may hold values from -0.09375 to 0.09375
- w_out: bfloat16 [2048, 4096], P('tp'), may hold values from -0.125 to 0.125
- sink: float32 [16], replicated, may hold values from 4 to 8
Outputs:
- mixed: bfloat16 [4096, 4096], P(('sp', 'tp'))
All inputs are finite; a program needn't handle non-finite values.
Results may differ from a plain program's by a relative error of at most 0.035.
Values may be sent and summed in bfloat16 or wider, within the bound.
A program may use at most 64 MiB of HBM per device.

v0:
```python
import jax
import jax.numpy as jnp
from jax import lax
from jax.sharding import PartitionSpec as P

HEAD_SIZE = 128
WINDOW_SIDE = 128
GRID_WIDTH = 64
EPS = 1e-05
THETA = 10000.0
MASKED = -1e30


def with_halo(cells, sides, width):
    for axis, dim in sides:
        count = lax.axis_size(axis)
        ends = count - 1
        head = lax.slice_in_dim(cells, 0, width, axis=dim)
        tail = lax.slice_in_dim(cells, cells.shape[dim] - width, cells.shape[dim], axis=dim)
        cells = jnp.concatenate(
            [
                lax.ppermute(tail, axis, [(i, (i + 1) % count) for i in range(ends)]),
                cells,
                lax.ppermute(head, axis, [((i + 1) % count, i) for i in range(ends)]),
            ],
            axis=dim,
        )
    return cells


def layer_norm(rows):
    values = rows.astype(jnp.float32)
    mean = jnp.mean(values, axis=-1, keepdims=True)
    var = jnp.mean(jnp.square(values - mean), axis=-1, keepdims=True)
    return (values - mean) * lax.rsqrt(var + EPS)


def rotate_half(values, token_position, width):
    half = width // 2
    inverse = THETA ** (-jnp.arange(half, dtype=jnp.float32) * 2.0 / width)
    angle = token_position.astype(jnp.float32)[:, None] * inverse[None, :]
    cosine = jnp.cos(angle)[:, None, :]
    sine = jnp.sin(angle)[:, None, :]
    first = values[..., :half]
    second = values[..., half:]
    return jnp.concatenate(
        [first * cosine - second * sine, second * cosine + first * sine], axis=-1
    )


def axial_rotation(heads, token_position, grid):
    width = heads.shape[-1] // 2
    values = heads.astype(jnp.float32)
    turned = jnp.concatenate(
        [
            rotate_half(values[..., :width], token_position // grid, width),
            rotate_half(values[..., width:], token_position % grid, width),
        ],
        axis=-1,
    )
    return turned.astype(jnp.bfloat16)


def sink_weights(scores, sink_column):
    top = jnp.maximum(jnp.max(scores, axis=-1, keepdims=True), sink_column)
    expo = jnp.exp(scores - top)
    return (expo / (jnp.sum(expo, axis=-1, keepdims=True) + jnp.exp(sink_column - top))).astype(
        jnp.bfloat16
    )


def shards(
    latent,
    context,
    cond,
    ctx_cond,
    w_shift,
    w_scale,
    w_gate,
    w_query,
    key_weight,
    value_weight,
    w_out,
    sink,
):
    sp_count = lax.axis_size("sp")
    sp_index = lax.axis_index("sp")
    tp_index = lax.axis_index("tp")
    block_rows = w_shift.shape[0]
    act = jax.nn.silu(jnp.stack([cond, ctx_cond])).astype(jnp.bfloat16)
    own_act = lax.dynamic_slice_in_dim(act, sp_index * block_rows, block_rows, 1)
    shift_part = jnp.dot(own_act, w_shift, preferred_element_type=jnp.float32)
    scale_part = jnp.dot(own_act, w_scale, preferred_element_type=jnp.float32)
    gate_part = jnp.dot(own_act[0:1], w_gate, preferred_element_type=jnp.float32)
    shift_sum, scale_sum, gate_sum = lax.psum((shift_part, scale_part, gate_part), "sp")
    shift, scale, gate = (
        lax.all_gather(shift_sum, "tp", axis=1, tiled=True),
        lax.all_gather(scale_sum, "tp", axis=1, tiled=True),
        lax.all_gather(gate_sum, "tp", axis=1, tiled=True),
    )
    latent_mod = (layer_norm(latent) * (1.0 + scale[0]) + shift[0]).astype(jnp.bfloat16)
    ctx_mod = (layer_norm(context) * (1.0 + scale[1]) + shift[1]).astype(jnp.bfloat16)
    kv_cols = key_weight.shape[1]
    q_cols = w_query.shape[1]
    ctx_pair = lax.all_gather(
        jnp.concatenate(
            [
                jnp.dot(ctx_mod, key_weight, preferred_element_type=jnp.float32).astype(
                    jnp.bfloat16
                ),
                jnp.dot(ctx_mod, value_weight, preferred_element_type=jnp.float32).astype(
                    jnp.bfloat16
                ),
            ],
            axis=1,
        ),
        "sp",
        axis=0,
        tiled=True,
    )
    piece = lax.all_gather(latent_mod, "tp", axis=0, tiled=True)
    projected_rows = jnp.concatenate(
        [
            jnp.dot(piece, w_query, preferred_element_type=jnp.float32).astype(jnp.bfloat16),
            jnp.dot(piece, key_weight, preferred_element_type=jnp.float32).astype(jnp.bfloat16),
            jnp.dot(piece, value_weight, preferred_element_type=jnp.float32).astype(jnp.bfloat16),
        ],
        axis=1,
    )
    tokens_here = projected_rows.shape[0]
    kv_heads = kv_cols // HEAD_SIZE
    q_heads = q_cols // HEAD_SIZE
    query_group = q_heads // kv_heads
    offset = sp_index * tokens_here
    token_position = offset + jnp.arange(tokens_here, dtype=jnp.int32)
    query = axial_rotation(
        projected_rows[:, :q_cols].reshape(tokens_here, q_heads, HEAD_SIZE),
        token_position,
        GRID_WIDTH,
    )
    key = axial_rotation(
        projected_rows[:, q_cols : q_cols + kv_cols].reshape(tokens_here, kv_heads, HEAD_SIZE),
        token_position,
        GRID_WIDTH,
    )
    value_rows = projected_rows[:, q_cols + kv_cols :]
    extended = with_halo(
        jnp.concatenate([key.reshape(tokens_here, kv_cols), value_rows], axis=1),
        (("sp", 0),),
        WINDOW_SIDE,
    )
    block_list = tokens_here // WINDOW_SIDE
    band = jnp.concatenate(
        [
            extended[shift_index * WINDOW_SIDE : shift_index * WINDOW_SIDE + tokens_here].reshape(
                block_list, WINDOW_SIDE, 2 * kv_cols
            )
            for shift_index in range(3)
        ],
        axis=1,
    )
    band_key = band[..., :kv_cols].reshape(block_list, 3 * WINDOW_SIDE, kv_heads, HEAD_SIZE)
    band_value = band[..., kv_cols:].reshape(block_list, 3 * WINDOW_SIDE, kv_heads, HEAD_SIZE)
    context_key_rows = ctx_pair[:, :kv_cols].reshape(-1, kv_heads, HEAD_SIZE)
    context_value_rows = ctx_pair[:, kv_cols:].reshape(-1, kv_heads, HEAD_SIZE)
    query_block_list = query.reshape(block_list, WINDOW_SIDE, kv_heads, query_group, HEAD_SIZE)
    factor = HEAD_SIZE ** (-0.5)
    band_scores = (
        jnp.einsum(
            "nqhgd,nkhd->nhgqk", query_block_list, band_key, preferred_element_type=jnp.float32
        )
        * factor
    )
    total = tokens_here * sp_count
    qpos = token_position.reshape(block_list, WINDOW_SIDE)[:, :, None]
    kpos = (
        offset
        - WINDOW_SIDE
        + (jnp.arange(block_list, dtype=jnp.int32) * WINDOW_SIDE)[:, None, None]
        + jnp.arange(3 * WINDOW_SIDE, dtype=jnp.int32)[None, None, :]
    )
    valid = (jnp.abs(kpos - qpos) <= WINDOW_SIDE) & (kpos >= 0) & (kpos < total)
    band_scores = jnp.where(valid[:, None, None], band_scores, MASKED)
    ctx_scores = (
        jnp.einsum(
            "nqhgd,khd->nhgqk",
            query_block_list,
            context_key_rows,
            preferred_element_type=jnp.float32,
        )
        * factor
    )
    own_sink = lax.dynamic_slice_in_dim(sink, tp_index * q_heads, q_heads).reshape(
        kv_heads, query_group
    )[:, :, None, None]
    weights = sink_weights(jnp.concatenate([band_scores, ctx_scores], axis=-1), own_sink)
    attended = jnp.einsum(
        "nhgqk,nkhd->nqhgd",
        weights[..., : 3 * WINDOW_SIDE],
        band_value,
        preferred_element_type=jnp.float32,
    ) + jnp.einsum(
        "nhgqk,khd->nqhgd",
        weights[..., 3 * WINDOW_SIDE :],
        context_value_rows,
        preferred_element_type=jnp.float32,
    )
    attended = attended.astype(jnp.bfloat16).reshape(tokens_here, q_cols)
    projected = lax.psum_scatter(
        jnp.dot(attended, w_out, preferred_element_type=jnp.float32).astype(jnp.bfloat16),
        "tp",
        scatter_dimension=0,
        tiled=True,
    ).astype(jnp.float32)
    return (latent.astype(jnp.float32) + gate[0][None, :] * projected).astype(jnp.bfloat16)


def solution(mesh):
    in_specs = (
        P(("sp", "tp"), None),
        P("sp", None),
        P(),
        P(),
        P("sp", "tp"),
        P("sp", "tp"),
        P("sp", "tp"),
        P(None, "tp"),
        P(None, "tp"),
        P(None, "tp"),
        P("tp", None),
        P(),
    )
    out_specs = P(("sp", "tp"), None)
    return jax.shard_map(shards, mesh=mesh, in_specs=in_specs, out_specs=out_specs, check_vma=False)
```

profile of v0, /device:TPU:0, one launch (start us, length us, event | category | flops | bytes accessed | tf_op | source)
XLA Modules:
  0.0 259.0 jit_solution(11385487950224661711)
XLA Ops:
  11.9 38.9 %all-reduce = (f32[2,1024]{1,0:T(2,128)S(1)}, f32[2,1024]{1,0:T(2,128)S(1)}, f32[1,1024]{1,0:T(1,128)S(1)}) all-reduce(f32[2,1024]{1,0:T(2,128)S(1)} %fusion.55, f32[2,1024]{1,0:T(2,128)S(1)} %fusion.54, f32[1,1024]{1,0:T(1,128)S(1)} %fusion.42), channel_id=1, replica_groups=mesh['sp'=8,'tp'=4] {'sp'}, use_global_device_ids=true, to_apply=%region_4.5 | all-reduce | flops 5120 | bytes 40960 | tf_op jit(solution)/shard_map/psum | solution.py:95
  50.8 5.2 %all_gather.17 = f32[2,4096]{1,0:T(2,128)S(1)} all-gather(f32[2,1024]{1,0:T(2,128)S(1)} %get-tuple-element.5), channel_id=1, replica_groups=mesh['sp'=8,'tp'=4] {'tp'}, dimensions={1}, use_global_device_ids=true | all-gather | bytes 40960 | tf_op jit(solution)/shard_map/all_gather | solution.py:97
  56.0 5.2 %all_gather.16 = f32[2,4096]{1,0:T(2,128)S(1)} all-gather(f32[2,1024]{1,0:T(2,128)S(1)} %get-tuple-element.6), channel_id=1, replica_groups=mesh['sp'=8,'tp'=4] {'tp'}, dimensions={1}, use_global_device_ids=true | all-gather | bytes 40960 | tf_op jit(solution)/shard_map/all_gather | solution.py:98
  61.9 2.2 convolution_convert_fusion.4
  71.4 1.9 fusion.32
  73.4 29.7 %all-gather.5.cloned.1.call-done = bf16[1024,512]{1,0:T(8,128)(2,1)} async-done(((bf16[128,512]{1,0:T(8,128)(2,1)}), bf16[1024,512]{1,0:T(8,128)(2,1)}) %all-gather.5.cloned.1.call-update) | async-done | bytes 1048592 | tf_op jit(solution)/shard_map/all_gather | solution.py:105
  103.1 2.3 fusion.49
  105.3 2.0 copy.150
  107.4 2.0 reshape.310
  109.4 28.5 %all-gather.3.cloned.1.call-done = bf16[512,4096]{1,0:T(8,128)(2,1)} async-done(((bf16[128,4096]{1,0:T(8,128)(2,1)}), bf16[512,4096]{1,0:T(8,128)(2,1)}) %all-gather.3.cloned.1.call-update) | async-done | bytes 4194320 | tf_op jit(solution)/shard_map/all_gather | solution.py:121
  137.9 5.9 %convolution_convert_fusion.1 = bf16[512,512]{0,1:T(8,128)(2,1)S(1)} fusion(bf16[512,4096]{1,0:T(8,128)(2,1)} %all-gather.3.cloned.1.call-done, bf16[4096,512]{1,0:T(8,128)(2,1)} %param.19), kind=kOutput, calls=%fused_computation.33 | convolution fusion | flops 2147745792 | bytes 8912896 | tf_op jit(solution)/shard_map/dot_general | solution.py:124
  152.7 3.5 %convolution_convert_fusion.3 = bf16[512,256]{0,1:T(8,128)(2,1)S(1)} fusion(bf16[512,4096]{1,0:T(8,128)(2,1)} %all-gather.3.cloned.1.call-done, bf16[4096,256]{1,0:T(8,128)(2,1)S(1)} %copy-done), kind=kOutput, calls=%fused_computation.36 | convolution fusion | flops 1073872896 | bytes 6553600 | tf_op jit(solution)/shard_map/dot_general | solution.py:125
  157.3 1.7 multiply_subtract_fusion
  162.2 3.0 %convolution_convert_fusion.2 = bf16[512,256]{1,0:T(8,128)(2,1)S(1)} fusion(bf16[512,4096]{1,0:T(8,128)(2,1)S(1)} %copy-done.17, bf16[4096,256]{1,0:T(8,128)(2,1)} %param.21), kind=kOutput, calls=%fused_computation.35 | convolution fusion | flops 1073872896 | bytes 6553600 | tf_op jit(solution)/shard_map/dot_general | solution.py:126
  165.3 3.5 %collective-permute-start = (bf16[128,512]{1,0:T(8,128)(2,1)S(1)}, bf16[128,512]{1,0:T(8,128)(2,1)S(1)}, u32[]{:S(2)}, u32[]{:S(2)}) collective-permute-start(bf16[128,512]{1,0:T(8,128)(2,1)S(1)} %get-tuple-element.24), channel_id=1, source_target_pairs={{0,4},{4,8},{8,12},{12,16},{16,20},{20,24},{24,28},{1,5},{5,9},{9,... | collective-permute-start | bytes 393224 | tf_op jit(solution)/shard_map/ppermute | solution.py:22
  171.0 4.5 %fusion.52 = (f32[4,2,2,128]{3,2,0,1:T(2,128)S(1)}, f32[4,2,2,128,1024]{3,4,2,0,1:T(8,128)}) fusion(bf16[4,128,2,2,128]{4,1,3,2,0:T(8,128)(2,1)S(1)} %pad_maximum_fusion.5, bf16[1024,2,128,1,1]{2,1,0,4,3:T(2,128)(2,1)S(1)} %bitcast.86), kind=kOutput, calls=%fused_computation.104 | convolution fusion | flops 541063168 | bytes 9445376 | tf_op jit(solution)/shard_map/nqhgd,khd->nhgqk/dot_general | solution.py:185
  180.9 6.0 %fusion.1 = f32[4,2,2,128]{3,2,0,1:T(2,128)S(1)} fusion(f32[4,2,2,128,1024]{3,4,2,0,1:T(8,128)} %get-tuple-element.43, f32[4,2,2,128]{3,2,0,1:T(2,128)S(1)} %copy.132, f32[4,2,2,128,384]{3,4,2,1,0:T(8,128)S(1)} %get-tuple-element.45), kind=kLoop, calls=%fused_computation.4 | loop fusion | flops 8648704 | bytes 11550720 | tf_op jit(solution)/shard_map/reduce_sum | solution.py:67
  187.1 4.6 %divide_convert_fusion = bf16[4,2,2,128,1408]{3,4,2,0,1:T(8,128)(2,1)} fusion(f32[4,2,2,128,1024]{3,4,2,0,1:T(8,128)S(1)} %bitcast.78, f32[4,2,2,128]{3,2,0,1:T(2,128)S(1)} %copy.134, f32[4,2,2,128]{3,2,0,1:T(2,128)S(1)} %copy.132, f32[4,2,2,128,384]{3,4,2,1,0:T(8,128)S(1)} %get-tuple-element.45), kind=kLoop, calls=%fused_computation.2 | loop fusion | flops 11534336 | bytes 17317888 | tf_op jit(solution)/shard_map/convert_element_type | solution.py:67
  192.1 2.9 %fusion.22 = f32[4,128,2,2,128]{1,4,3,2,0:T(8,128)S(1)} fusion(bf16[1024,2,128,1,1]{0,2,4,1,3:T(8,128)(2,1)S(1)} %bitcast.90, bf16[4,2,2,128,1408]{3,4,2,0,1:T(8,128)(2,1)} %divide_convert_fusion), kind=kOutput, calls=%fused_computation.31 | convolution fusion | flops 536870912 | bytes 5767168 | tf_op jit(solution)/shard_map/nhgqk,khd->nqhgd/dot_general | solution.py:202
  195.0 1.9 fusion.28
  197.5 6.5 %convolution_convert_fusion = bf16[512,4096]{1,0:T(8,128)(2,1)} fusion(bf16[512,512]{1,0:T(8,128)(2,1)S(1)} %reshape.312, bf16[512,4096]{1,0:T(8,128)(2,1)} %param.22), kind=kOutput, calls=%fused_computation.5 | convolution fusion | flops 2149580800 | bytes 8912896 | tf_op jit(solution)/shard_map/dot_general | solution.py:210
  204.0 5.3 %all_gather.15 = f32[1,4096]{1,0:T(1,128)S(1)} all-gather(f32[1,1024]{1,0:T(1,128)S(1)} %get-tuple-element.7), channel_id=1, replica_groups=mesh['sp'=8,'tp'=4] {'tp'}, dimensions={1}, use_global_device_ids=true | all-gather | bytes 20480 | tf_op jit(solution)/shard_map/all_gather | solution.py:99
  209.4 40.6 %reduce-scatter.2.cloned.1.call-done = bf16[128,4096]{1,0:T(8,128)(2,1)} async-done(((bf16[512,4096]{1,0:T(8,128)(2,1)}), bf16[128,4096]{1,0:T(8,128)(2,1)}) %reduce-scatter.2.cloned.1.call-update) | async-done | bytes 1048592 | tf_op jit(solution)/shard_map/reduce_scatter | solution.py:209
  249.9 2.5 fusion.16
  (115 shorter events, 35.1 us)
Async XLA Ops:
  6.5 57.6 %copy-start = (bf16[4096,256]{1,0:T(8,128)(2,1)S(1)}, bf16[4096,256]{1,0:T(8,128)(2,1)}, u32[]{:S(2)}) copy-start(bf16[4096,256]{1,0:T(8,128)(2,1)} %param.20) | copy-start | bytes 6291460
  6.5 54.7 %copy-start.3 = (bf16[128,4096]{1,0:T(8,128)(2,1)S(1)}, bf16[128,4096]{1,0:T(8,128)(2,1)}, u32[]{:S(2)}) copy-start(bf16[128,4096]{1,0:T(8,128)(2,1)} %param.13) | copy-start | bytes 3145732
  6.5 96.6 %all-gather.5.cloned.1.call-start = ((), (), s32[]{:S(2)}) async-start(), calls=%async_computation.2 | async-start | bytes 1179648 | tf_op jit(solution)/shard_map/all_gather | solution.py:105
  61.5 2.6 %copy-start.4 = (bf16[128,4096]{1,0:T(8,128)(2,1)S(1)}, bf16[128,4096]{1,0:T(8,128)(2,1)}, u32[]{:S(2)}) copy-start(bf16[128,4096]{1,0:T(8,128)(2,1)} %param.13) | copy-start | bytes 3145732
  65.4 72.4 %all-gather.3.cloned.1.call-start = ((), (), s32[]{:S(2)}) async-start(), calls=%async_computation.1 | async-start | bytes 5242880 | tf_op jit(solution)/shard_map/all_gather | solution.py:121
  65.7 5.4 %copy-start.18 = (f32[16]{0:T(128)S(1)}, f32[16]{0:T(128)}, u32[]{:S(2)}) copy-start(f32[16]{0:T(128)} %param.23) | copy-start | bytes 196
  67.6 182.3 %reduce-scatter.2.cloned.1.call-start = ((), (), s32[]{:S(2)}) async-start(), calls=%async_computation.3 | async-start | bytes 5242880 | tf_op jit(solution)/shard_map/reduce_scatter | solution.py:209
  68.4 1.7 copy-start.12
  137.8 6.0 %copy-start.13 = (f32[512,32]{0,1:T(8,128)S(1)}, f32[512,32]{0,1:T(8,128)}, u32[]{:S(2)}) copy-start(f32[512,32]{0,1:T(8,128)} %copy-done.12) | copy-start | bytes 196612
  137.9 6.0 %copy-start.15 = (f32[512,32]{0,1:T(8,128)S(1)}, f32[512,32]{0,1:T(8,128)}, u32[]{:S(2)}) copy-start(f32[512,32]{0,1:T(8,128)} %copy-done.14) | copy-start | bytes 196612
  157.3 4.9 %copy-start.17 = (bf16[512,4096]{1,0:T(8,128)(2,1)S(1)}, bf16[512,4096]{1,0:T(8,128)(2,1)}, u32[]{:S(2)}) copy-start(bf16[512,4096]{1,0:T(8,128)(2,1)} %all-gather.3.cloned.1.call-done) | copy-start | bytes 12582916
  162.2 8.1 %copy-start.6 = (bf16[4,128,2,2,32]{4,1,3,2,0:T(8,128)(2,1)S(1)}, bf16[4,128,2,2,32]{4,1,3,2,0:T(8,128)(2,1)}, u32[]{:S(2)}) copy-start(bf16[4,128,2,2,32]{4,1,3,2,0:T(8,128)(2,1)} %copy.125) | copy-start | bytes 393220
  162.2 8.1 %copy-start.7 = (bf16[4,128,2,2,32]{4,1,3,2,0:T(8,128)(2,1)S(1)}, bf16[4,128,2,2,32]{4,1,3,2,0:T(8,128)(2,1)}, u32[]{:S(2)}) copy-start(bf16[4,128,2,2,32]{4,1,3,2,0:T(8,128)(2,1)} %copy.124) | copy-start | bytes 393220
  162.2 8.1 %copy-start.8 = (bf16[4,128,2,2,32]{4,1,3,2,0:T(8,128)(2,1)S(1)}, bf16[4,128,2,2,32]{4,1,3,2,0:T(8,128)(2,1)}, u32[]{:S(2)}) copy-start(bf16[4,128,2,2,32]{4,1,3,2,0:T(8,128)(2,1)} %copy.123) | copy-start | bytes 393220
  162.2 8.1 %copy-start.9 = (bf16[4,128,2,2,32]{4,1,3,2,0:T(8,128)(2,1)S(1)}, bf16[4,128,2,2,32]{4,1,3,2,0:T(8,128)(2,1)}, u32[]{:S(2)}) copy-start(bf16[4,128,2,2,32]{4,1,3,2,0:T(8,128)(2,1)} %copy.122) | copy-start | bytes 393220
  165.2 5.8 %copy-start.10 = (bf16[1024,2,128]{2,1,0:T(2,128)(2,1)S(1)}, bf16[1024,2,128]{2,1,0:T(2,128)(2,1)}, u32[]{:S(2)}) copy-start(bf16[1024,2,128]{2,1,0:T(2,128)(2,1)} %reshape.310) | copy-start | bytes 1572868
  165.3 10.5 %collective-permute-start = (bf16[128,512]{1,0:T(8,128)(2,1)S(1)}, bf16[128,512]{1,0:T(8,128)(2,1)S(1)}, u32[]{:S(2)}, u32[]{:S(2)}) collective-permute-start(bf16[128,512]{1,0:T(8,128)(2,1)S(1)} %get-tuple-element.24), channel_id=1, source_target_pairs={{0,4},{4,8},{8,12},{12,16},{16,20},{20,24},{24,28},{1,5},{5,9},{9,... | collective-permute-start | bytes 393224 | tf_op jit(solution)/shard_map/ppermute | solution.py:22
  168.8 7.4 %collective-permute-start.1 = (bf16[128,512]{1,0:T(8,128)(2,1)S(1)}, bf16[128,512]{1,0:T(8,128)(2,1)}, u32[]{:S(2)}, u32[]{:S(2)}) collective-permute-start(bf16[128,512]{1,0:T(8,128)(2,1)S(1)} %get-tuple-element.25), channel_id=1, source_target_pairs={{4,0},{8,4},{12,8},{16,12},{20,16},{24,20},{28,24},{5,1},{9,5},{13... | collective-permute-start | bytes 393224 | tf_op jit(solution)/shard_map/ppermute | solution.py:24
  177.2 2.8 %copy-start.11 = (pred[4,128,384]{1,2,0:T(8,128)(4,1)S(1)}, pred[4,128,384]{1,2,0:T(8,128)(4,1)}, u32[]{:S(2)}) copy-start(pred[4,128,384]{1,2,0:T(8,128)(4,1)} %fusion.32) | copy-start | bytes 589828
  180.1 6.9 %slice-start = ((s8[8388608]{0:T(1024)(128)(4,1)}), s8[4194304]{0:T(1024)(128)(4,1)S(1)}, s32[]{:S(2)}) async-start(s8[8388608]{0:T(1024)(128)(4,1)} %bitcast.77), calls=%async_computation.4 | async-start | bytes 8388608
  180.9 6.1 %slice-start.1 = ((s8[8388608]{0:T(1024)(128)(4,1)}), s8[4194304]{0:T(1024)(128)(4,1)S(1)}, s32[]{:S(2)}) async-start(s8[8388608]{0:T(1024)(128)(4,1)} %bitcast.77), calls=%async_computation.5 | async-start | bytes 8388608
  187.0 4.7 %copy-start.5 = (bf16[4,384,256]{2,1,0:T(8,128)(2,1)S(1)}, bf16[4,384,256]{2,1,0:T(8,128)(2,1)}, u32[]{:S(2)}) copy-start(bf16[4,384,256]{2,1,0:T(8,128)(2,1)} %get-tuple-element.8) | copy-start | bytes 2359300
  187.1 5.0 %copy-start.16 = (bf16[1024,256]{0,1:T(8,128)(2,1)S(1)}, bf16[1024,256]{0,1:T(8,128)(2,1)}, u32[]{:S(2)}) copy-start(bf16[1024,256]{0,1:T(8,128)(2,1)} %copy.150) | copy-start | bytes 1572868
  204.0 48.4 %copy-start.1 = (bf16[4096,256]{1,0:T(8,128)(2,1)S(1)}, bf16[4096,256]{1,0:T(8,128)(2,1)}, u32[]{:S(2)}) copy-start(bf16[4096,256]{1,0:T(8,128)(2,1)} %param.20) | copy-start | bytes 6291460
  (2 other events, 3.0 us)
Sparse Core Ops, SparseCore 0:
  65.5 37.5 all-gather.4
  104.6 33.1 all-gather.2
  204.2 45.7 reduce-scatter.1
where the time goes:
time: 260 us; the launch traced here: 259 us
  waiting for transfers between devices  99.3 us (38%)
  blocking collectives  54.6 us (21%)
  matrix products  36 us (14%)
  other arithmetic  28.1 us (11%)
  local copies, waits for them, and re-layouts  22.1 us (8%)
  between operations  13.6 us (5%)
  starting transfers between devices  5.29 us (2%)
    reduce_scatter x1, waiting for transfers between devices, shards(): lax.psum_scatter(jnp.dot(attended, w_out, preferred_element_type=jnp.floa...  40.6 us
    psum x1, blocking collectives, shards(): lax.psum((shift_part, scale_part, gate_part), 'sp')  38.9 us
    all_gather x1, waiting for transfers between devices, shards(): lax.all_gather(jnp.concatenate([jnp.dot(ctx_mod, key_weight, preferred_el...  29.7 us
    all_gather x1, waiting for transfers between devices, shards(): piece = lax.all_gather(latent_mod, 'tp', axis=0, tiled=True)  28.5 us
    concatenate x8, local copies, waits for them, and re-layouts, axial_rotation(): jnp.concatenate([rotate_half(values[..., :width], token_position // grid,...  7.91 us
    dot_general x1, matrix products, shards(): jnp.dot(attended, w_out, preferred_element_type=jnp.float32)  6.47 us
    reduce_sum x1, other arithmetic, sink_weights(): jnp.sum(expo, axis=-1, keepdims=True) + jnp.exp(sink_column - top)  6.03 us
    dot_general x1, matrix products, shards(): jnp.dot(piece, w_query, preferred_element_type=jnp.float32)  5.86 us
  transfers between devices with their start and end apart: 5, of which 4 were waited for; matrix products, arithmetic and copies ran while one was open for 7% of the time, Pallas kernels for 0%

commit v1 on v0

--- a/solution.py
+++ b/solution.py
@@ -118,7 +118,12 @@
         axis=0,
         tiled=True,
     )
-    piece = lax.all_gather(latent_mod, "tp", axis=0, tiled=True)
+    ring = [latent_mod]
+    for hop in range(3):
+        ring.append(lax.ppermute(ring[-1], "tp", [(dev, (dev + 1) % 4) for dev in range(4)]))
+    piece = jnp.roll(
+        jnp.concatenate(ring[::-1], axis=0), (lax.axis_index("tp") + 1) * ring[0].shape[0], axis=0
+    )
     projected_rows = jnp.concatenate(
         [
             jnp.dot(piece, w_query, preferred_element_type=jnp.float32).astype(jnp.bfloat16),

time: 260 us -> 252 us (0.969)
  waiting for transfers between devices: 99.3 us -> 84 us
  local copies, waits for them, and re-layouts: 22.1 us -> 32.3 us
  matrix products: 36 us -> 30.3 us
  other arithmetic: 28.1 us -> 31 us
    all_gather x1 -> x0, waiting for transfers between devices: 28.5 us -> none  [shards(): piece = lax.all_gather(latent_mod, 'tp', axis=0, tiled=True)]
    ppermute x0 -> x3, waiting for transfers between devices: none -> 21.3 us  [shards(): lax.ppermute(ring[-1], 'tp', [(dev, (dev + 1) % 4) for dev in range(4)])]
    unnamed x47, local copies, waits for them, and re-layouts: 1.07 us -> 12.4 us
    all_gather x1, waiting for transfers between devices: 29.7 us -> 22.3 us  [shards(): lax.all_gather(jnp.concatenate([jnp.dot(ctx_mod, key_weight, preferred_el...]
    concatenate x8, local copies, waits for them, and re-layouts: 7.91 us -> 4.6 us  [axial_rotation(): jnp.concatenate([rotate_half(values[..., :width], token_position // grid,...]
  transfers between devices with their start and end apart: 5 -> 7, of which waited for: 4 -> 4; matrix products, arithmetic and copies ran while one was open for 7% -> 13% of each run, Pallas kernels for 0% -> 0%
where the time goes in v1:
time: 252 us; the launch traced here: 251 us
  waiting for transfers between devices  84 us (33%)
  blocking collectives  54.7 us (22%)
  local copies, waits for them, and re-layouts  32.3 us (13%)
  other arithmetic  31 us (12%)
  matrix products  30.3 us (12%)
  between operations  13.9 us (6%)
  starting transfers between devices  5.2 us (2%)
    reduce_scatter x1, waiting for transfers between devices, shards(): lax.psum_scatter(jnp.dot(attended, w_out, preferred_element_type=jnp.floa...  40.5 us
    psum x1, blocking collectives, shards(): lax.psum((shift_part, scale_part, gate_part), 'sp')  38.9 us
    all_gather x1, waiting for transfers between devices, shards(): lax.all_gather(jnp.concatenate([jnp.dot(ctx_mod, key_weight, preferred_el...  22.3 us
    ppermute x3, waiting for transfers between devices, shards(): lax.ppermute(ring[-1], 'tp', [(dev, (dev + 1) % 4) for dev in range(4)])  21.3 us
    unnamed x47, local copies, waits for them, and re-layouts  12.4 us
    dot_general x1, matrix products, shards(): jnp.dot(attended, w_out, preferred_element_type=jnp.float32)  6.49 us
    reduce_sum x1, other arithmetic, sink_weights(): jnp.sum(expo, axis=-1, keepdims=True) + jnp.exp(sink_column - top)  6.03 us
    dot_general x1, matrix products, shards(): jnp.einsum('nqhgd,khd->nhgqk', query_block_list, context_key_rows, prefer...  5.54 us
  transfers between devices with their start and end apart: 7, of which 4 were waited for; matrix products, arithmetic and copies ran while one was open for 13% of the time, Pallas kernels for 0%

profile of v1, /device:TPU:0, one launch (start us, length us, event | category | flops | bytes accessed | tf_op | source)
XLA Modules:
  0.0 251.4 jit_solution(3164213883459555789)
XLA Ops:
  11.9 38.9 %all-reduce = (f32[2,1024]{1,0:T(2,128)S(1)}, f32[2,1024]{1,0:T(2,128)S(1)}, f32[1,1024]{1,0:T(1,128)S(1)}) all-reduce(f32[2,1024]{1,0:T(2,128)S(1)} %fusion.73, f32[2,1024]{1,0:T(2,128)S(1)} %fusion.72, f32[1,1024]{1,0:T(1,128)S(1)} %fusion.57), channel_id=1, replica_groups=mesh['sp'=8,'tp'=4] {'sp'}, use_global_device_ids=true, to_apply=%region_4.5 | all-reduce | flops 5120 | bytes 40960 | tf_op jit(solution)/shard_map/psum | solution.py:95
  50.8 5.3 %all_gather.13 = f32[2,4096]{1,0:T(2,128)S(1)} all-gather(f32[2,1024]{1,0:T(2,128)S(1)} %get-tuple-element.6), channel_id=1, replica_groups=mesh['sp'=8,'tp'=4] {'tp'}, dimensions={1}, use_global_device_ids=true | all-gather | bytes 40960 | tf_op jit(solution)/shard_map/all_gather | solution.py:98
  56.2 5.2 %all_gather.14 = f32[2,4096]{1,0:T(2,128)S(1)} all-gather(f32[2,1024]{1,0:T(2,128)S(1)} %get-tuple-element.5), channel_id=1, replica_groups=mesh['sp'=8,'tp'=4] {'tp'}, dimensions={1}, use_global_device_ids=true | all-gather | bytes 40960 | tf_op jit(solution)/shard_map/all_gather | solution.py:97
  65.4 11.6 %collective-permute-done = bf16[128,4096]{1,0:T(8,128)(2,1)} collective-permute-done((bf16[128,4096]{1,0:T(8,128)(2,1)S(1)}, bf16[128,4096]{1,0:T(8,128)(2,1)}, u32[]{:S(2)}, u32[]{:S(2)}) %collective-permute-start) | collective-permute-done | bytes 1048608 | tf_op jit(solution)/shard_map/ppermute | solution.py:123
  81.8 9.7 %collective-permute-done.1 = bf16[128,4096]{1,0:T(8,128)(2,1)} collective-permute-done((bf16[128,4096]{1,0:T(8,128)(2,1)}, bf16[128,4096]{1,0:T(8,128)(2,1)}, u32[]{:S(2)}, u32[]{:S(2)}) %collective-permute-start.1) | collective-permute-done | bytes 1048608 | tf_op jit(solution)/shard_map/ppermute | solution.py:123
  91.6 1.9 fusion.47
  93.5 22.3 %all-gather.2.cloned.1.call-done = bf16[1024,512]{1,0:T(8,128)(2,1)} async-done(((bf16[128,512]{1,0:T(8,128)(2,1)}), bf16[1024,512]{1,0:T(8,128)(2,1)}) %all-gather.2.cloned.1.call-update) | async-done | bytes 1048592 | tf_op jit(solution)/shard_map/all_gather | solution.py:105
  115.8 2.2 fusion.67
  118.1 2.0 reshape.310
  120.1 2.0 copy.150
  132.3 2.2 copy-done.11
  138.3 1.7 multiply_subtract_fusion.1
  144.0 3.1 %collective-permute-start.3 = (bf16[128,512]{1,0:T(8,128)(2,1)}, bf16[128,512]{1,0:T(8,128)(2,1)}, u32[]{:S(2)}, u32[]{:S(2)}) collective-permute-start(bf16[128,512]{1,0:T(8,128)(2,1)} %get-tuple-element.24), channel_id=1, source_target_pairs={{0,4},{4,8},{8,12},{12,16},{16,20},{20,24},{24,28},{1,5},{5,9},{9,... | collective-permute-start | bytes 393224 | tf_op jit(solution)/shard_map/ppermute | solution.py:22
  148.8 4.6 %fusion.34 = bf16[512,512]{0,1:T(8,128)(2,1)S(1)} fusion(bf16[4096,512]{1,0:T(8,128)(2,1)S(1)} %copy-done.12, bf16[1024,4096]{1,0:T(8,128)(2,1)} %copy-done.11, s32[]{:T(128)S(6)} %select_n.47), kind=kOutput, calls=%fused_computation.39 | convolution fusion | flops 2147745792 | bytes 8912900 | tf_op jit(solution)/shard_map/dot_general | solution.py:129
  159.0 1.9 pad_maximum_fusion.5
  160.9 5.5 %fusion.70 = (f32[4,2,2,128]{3,2,0,1:T(2,128)S(1)}, f32[4,2,2,128,1024]{3,4,2,0,1:T(8,128)}) fusion(bf16[4,128,2,2,128]{4,1,3,2,0:T(8,128)(2,1)S(1)} %pad_maximum_fusion.5, bf16[1024,2,128,1,1]{2,1,0,4,3:T(2,128)(2,1)} %bitcast.83), kind=kOutput, calls=%fused_computation.121 | convolution fusion | flops 541063168 | bytes 9445376 | tf_op jit(solution)/shard_map/nqhgd,khd->nhgqk/dot_general | solution.py:190
  173.1 6.0 %fusion.1 = f32[4,2,2,128]{3,2,0,1:T(2,128)S(1)} fusion(f32[4,2,2,128,1024]{3,4,2,0,1:T(8,128)} %get-tuple-element.43, f32[4,2,2,128]{3,2,0,1:T(2,128)S(1)} %copy.132, f32[4,2,2,128,384]{3,4,2,1,0:T(8,128)S(1)} %get-tuple-element.45), kind=kLoop, calls=%fused_computation.4 | loop fusion | flops 8648704 | bytes 11550720 | tf_op jit(solution)/shard_map/reduce_sum | solution.py:67
  179.3 4.6 %divide_convert_fusion = bf16[4,2,2,128,1408]{3,4,2,0,1:T(8,128)(2,1)} fusion(f32[4,2,2,128,1024]{3,4,2,0,1:T(8,128)S(1)} %bitcast.75, f32[4,2,2,128]{3,2,0,1:T(2,128)S(1)} %copy.134, f32[4,2,2,128]{3,2,0,1:T(2,128)S(1)} %copy.132, f32[4,2,2,128,384]{3,4,2,1,0:T(8,128)S(1)} %get-tuple-element.45), kind=kLoop, calls=%fused_computation.2 | loop fusion | flops 11534336 | bytes 17317888 | tf_op jit(solution)/shard_map/convert_element_type | solution.py:67
  184.3 2.9 %fusion.28 = f32[4,128,2,2,128]{1,4,3,2,0:T(8,128)S(1)} fusion(bf16[1024,2,128,1,1]{0,2,4,1,3:T(8,128)(2,1)S(1)} %bitcast.87, bf16[4,2,2,128,1408]{3,4,2,0,1:T(8,128)(2,1)} %divide_convert_fusion), kind=kOutput, calls=%fused_computation.37 | convolution fusion | flops 536870912 | bytes 5767168 | tf_op jit(solution)/shard_map/nhgqk,khd->nqhgd/dot_general | solution.py:207
  187.2 1.9 fusion.37
  189.7 6.5 %convolution_convert_fusion = bf16[512,4096]{1,0:T(8,128)(2,1)} fusion(bf16[512,512]{1,0:T(8,128)(2,1)S(1)} %reshape.312, bf16[512,4096]{1,0:T(8,128)(2,1)} %param.22), kind=kOutput, calls=%fused_computation.5 | convolution fusion | flops 2149580800 | bytes 8912896 | tf_op jit(solution)/shard_map/dot_general | solution.py:215
  196.2 5.3 %all_gather.12 = f32[1,4096]{1,0:T(1,128)S(1)} all-gather(f32[1,1024]{1,0:T(1,128)S(1)} %get-tuple-element.7), channel_id=1, replica_groups=mesh['sp'=8,'tp'=4] {'tp'}, dimensions={1}, use_global_device_ids=true | all-gather | bytes 20480 | tf_op jit(solution)/shard_map/all_gather | solution.py:99
  201.6 40.5 %reduce-scatter.2.cloned.1.call-done = bf16[128,4096]{1,0:T(8,128)(2,1)} async-done(((bf16[512,4096]{1,0:T(8,128)(2,1)}), bf16[128,4096]{1,0:T(8,128)(2,1)}) %reduce-scatter.2.cloned.1.call-update) | async-done | bytes 1048592 | tf_op jit(solution)/shard_map/reduce_scatter | solution.py:214
  242.0 2.5 fusion.22
  (120 shorter events, 47.1 us)
Async XLA Ops:
  6.5 57.1 %copy-start = (bf16[4096,256]{1,0:T(8,128)(2,1)S(1)}, bf16[4096,256]{1,0:T(8,128)(2,1)}, u32[]{:S(2)}) copy-start(bf16[4096,256]{1,0:T(8,128)(2,1)} %param.20) | copy-start | bytes 6291460
  6.5 54.8 %copy-start.2 = (bf16[128,4096]{1,0:T(8,128)(2,1)S(1)}, bf16[128,4096]{1,0:T(8,128)(2,1)}, u32[]{:S(2)}) copy-start(bf16[128,4096]{1,0:T(8,128)(2,1)} %param.12) | copy-start | bytes 3145732
  6.5 109.3 %all-gather.2.cloned.1.call-start = ((), (), s32[]{:S(2)}) async-start(), calls=%async_computation.1 | async-start | bytes 1179648 | tf_op jit(solution)/shard_map/all_gather | solution.py:105
  50.8 12.1 %copy-start.3 = (bf16[128,4096]{1,0:T(8,128)(2,1)S(1)}, bf16[128,4096]{1,0:T(8,128)(2,1)}, u32[]{:S(2)}) copy-start(bf16[128,4096]{1,0:T(8,128)(2,1)} %param.13) | copy-start | bytes 3145732
  62.6 14.4 %collective-permute-start = (bf16[128,4096]{1,0:T(8,128)(2,1)S(1)}, bf16[128,4096]{1,0:T(8,128)(2,1)}, u32[]{:S(2)}, u32[]{:S(2)}) collective-permute-start(bf16[128,4096]{1,0:T(8,128)(2,1)S(1)} %fusion.17), channel_id=1, source_target_pairs={{0,1},{1,2},{2,3},{3,0},{4,5},{5,6},{6,7},{7,4},{8,9},{9,10},{10,1... | collective-permute-start | bytes 3145736 | tf_op jit(solution)/shard_map/ppermute | solution.py:123
  64.8 16.9 %copy-start.15 = (f32[16]{0:T(128)S(1)}, f32[16]{0:T(128)}, u32[]{:S(2)}) copy-start(f32[16]{0:T(128)} %param.23) | copy-start | bytes 196
  76.9 14.5 %collective-permute-start.1 = (bf16[128,4096]{1,0:T(8,128)(2,1)}, bf16[128,4096]{1,0:T(8,128)(2,1)}, u32[]{:S(2)}, u32[]{:S(2)}) collective-permute-start(bf16[128,4096]{1,0:T(8,128)(2,1)} %collective-permute-done), channel_id=1, source_target_pairs={{0,1},{1,2},{2,3},{3,0},{4,5},{5,6},{6,7},{7,4},{8,9},{9,10},{10,1... | collective-permute-start | bytes 3145736 | tf_op jit(solution)/shard_map/ppermute | solution.py:123
  77.6 164.4 %reduce-scatter.2.cloned.1.call-start = ((), (), s32[]{:S(2)}) async-start(), calls=%async_computation.2 | async-start | bytes 5242880 | tf_op jit(solution)/shard_map/reduce_scatter | solution.py:214
  78.3 45.2 %copy-start.6 = (f32[512,32]{0,1:T(8,128)}, f32[512,32]{0,1:T(8,128)S(1)}, u32[]{:S(2)}) copy-start(f32[512,32]{0,1:T(8,128)S(1)} %get-tuple-element.40) | copy-start | bytes 196612
  78.3 45.2 %copy-start.8 = (f32[512,32]{0,1:T(8,128)}, f32[512,32]{0,1:T(8,128)S(1)}, u32[]{:S(2)}) copy-start(f32[512,32]{0,1:T(8,128)S(1)} %get-tuple-element.41) | copy-start | bytes 196612
  91.5 30.6 %collective-permute-start.2 = (bf16[128,4096]{1,0:T(8,128)(2,1)}, bf16[128,4096]{1,0:T(8,128)(2,1)}, u32[]{:S(2)}, u32[]{:S(2)}) collective-permute-start(bf16[128,4096]{1,0:T(8,128)(2,1)} %collective-permute-done.1), channel_id=1, source_target_pairs={{0,1},{1,2},{2,3},{3,0},{4,5},{5,6},{6,7},{7,4},{8,9},{9,10},{10,1... | collective-permute-start | bytes 3145736 | tf_op jit(solution)/shard_map/ppermute | solution.py:123
  130.9 3.5 %copy-start.11 = (bf16[1024,4096]{1,0:T(8,128)(2,1)}, bf16[1024,4096]{1,0:T(8,128)(2,1)S(1)}, u32[]{:S(2)}) copy-start(bf16[1024,4096]{1,0:T(8,128)(2,1)S(1)} %constant_dynamic-update-slice_fusion) | copy-start | bytes 25165828
  130.9 3.5 %copy-start.14 = (bf16[4096,256]{1,0:T(8,128)(2,1)S(1)}, bf16[4096,256]{1,0:T(8,128)(2,1)}, u32[]{:S(2)}) copy-start(bf16[4096,256]{1,0:T(8,128)(2,1)} %param.21) | copy-start | bytes 6291460
  138.3 10.5 %copy-start.12 = (bf16[4096,512]{1,0:T(8,128)(2,1)S(1)}, bf16[4096,512]{1,0:T(8,128)(2,1)}, u32[]{:S(2)}) copy-start(bf16[4096,512]{1,0:T(8,128)(2,1)} %param.19) | copy-start | bytes 12582916
  144.0 23.3 %collective-permute-start.3 = (bf16[128,512]{1,0:T(8,128)(2,1)}, bf16[128,512]{1,0:T(8,128)(2,1)}, u32[]{:S(2)}, u32[]{:S(2)}) collective-permute-start(bf16[128,512]{1,0:T(8,128)(2,1)} %get-tuple-element.24), channel_id=1, source_target_pairs={{0,4},{4,8},{8,12},{12,16},{16,20},{20,24},{24,28},{1,5},{5,9},{9,... | collective-permute-start | bytes 393224 | tf_op jit(solution)/shard_map/ppermute | solution.py:22
  147.1 6.4 %copy-start.7 = (f32[512,32]{0,1:T(8,128)S(1)}, f32[512,32]{0,1:T(8,128)}, u32[]{:S(2)}) copy-start(f32[512,32]{0,1:T(8,128)} %copy-done.6) | copy-start | bytes 196612
  147.1 6.4 %copy-start.9 = (f32[512,32]{0,1:T(8,128)S(1)}, f32[512,32]{0,1:T(8,128)}, u32[]{:S(2)}) copy-start(f32[512,32]{0,1:T(8,128)} %copy-done.8) | copy-start | bytes 196612
  147.1 20.2 %collective-permute-start.4 = (bf16[128,512]{1,0:T(8,128)(2,1)}, bf16[128,512]{1,0:T(8,128)(2,1)}, u32[]{:S(2)}, u32[]{:S(2)}) collective-permute-start(bf16[128,512]{1,0:T(8,128)(2,1)} %get-tuple-element.25), channel_id=1, source_target_pairs={{4,0},{8,4},{12,8},{16,12},{20,16},{24,20},{28,24},{5,1},{9,5},{13... | collective-permute-start | bytes 393224 | tf_op jit(solution)/shard_map/ppermute | solution.py:24
  169.5 2.8 %copy-start.5 = (pred[4,128,384]{1,2,0:T(8,128)(4,1)S(1)}, pred[4,128,384]{1,2,0:T(8,128)(4,1)}, u32[]{:S(2)}) copy-start(pred[4,128,384]{1,2,0:T(8,128)(4,1)} %fusion.47) | copy-start | bytes 589828
  172.3 6.9 %slice-start = ((s8[8388608]{0:T(1024)(128)(4,1)}), s8[4194304]{0:T(1024)(128)(4,1)S(1)}, s32[]{:S(2)}) async-start(s8[8388608]{0:T(1024)(128)(4,1)} %bitcast.74), calls=%async_computation.3 | async-start | bytes 8388608
  173.1 6.1 %slice-start.1 = ((s8[8388608]{0:T(1024)(128)(4,1)}), s8[4194304]{0:T(1024)(128)(4,1)S(1)}, s32[]{:S(2)}) async-start(s8[8388608]{0:T(1024)(128)(4,1)} %bitcast.74), calls=%async_computation.4 | async-start | bytes 8388608
  179.3 4.6 %copy-start.4 = (bf16[4,384,256]{2,1,0:T(8,128)(2,1)S(1)}, bf16[4,384,256]{2,1,0:T(8,128)(2,1)}, u32[]{:S(2)}) copy-start(bf16[4,384,256]{2,1,0:T(8,128)(2,1)} %get-tuple-element.8) | copy-start | bytes 2359300
  179.3 5.0 %copy-start.10 = (bf16[1024,256]{0,1:T(8,128)(2,1)S(1)}, bf16[1024,256]{0,1:T(8,128)(2,1)}, u32[]{:S(2)}) copy-start(bf16[1024,256]{0,1:T(8,128)(2,1)} %copy.150) | copy-start | bytes 1572868
  196.2 48.3 %copy-start.1 = (bf16[4096,256]{1,0:T(8,128)(2,1)S(1)}, bf16[4096,256]{1,0:T(8,128)(2,1)}, u32[]{:S(2)}) copy-start(bf16[4096,256]{1,0:T(8,128)(2,1)} %param.20) | copy-start | bytes 6291460
  (1 other events, 1.6 us)
Sparse Core Ops, SparseCore 0:
  77.8 38.0 all-gather.1
  196.4 45.6 reduce-scatter.1
